TPU v7x, 32 devices: a whole 2x2x4 slice. The times are simulated.
32 devices in a mesh: fs: 16 (over z, y, x), tp: 2 (over core).
Axes of the slice: x: 2, y: 2, z: 4, core: 2. Of those that a mesh axis runs over, the one named last changes fastest.
Arguments:
- normed_input: bfloat16 [8192, 2048], P('fs', 'tp'), may hold values from -6 to 6
- cotangent: bfloat16 [8192, 2048], P('fs', 'tp'), may hold values from -6 to 6
- up_weight: bfloat16 [2048, 8192], P('fs', 'tp'), may hold values from -0.125 to 0.125
- down_weight: bfloat16 [8192, 2048], P('tp', 'fs'), may hold values from -0.0625 to 0.0625
Outputs:
- input_grad: bfloat16 [8192, 2048], P('fs', 'tp')
- up_grad: float32 [2048, 8192], P('fs', 'tp')
- down_grad: float32 [8192, 2048], P('tp', 'fs')
All inputs are finite; a program needn't handle non-finite values.
Results may differ from a plain program's by a relative error of at most 0.018.
Values may be sent and summed in bfloat16 or wider, within the bound.
A program may use at most 192 MiB of HBM per device.

v0:
```python
import jax
import jax.numpy as jnp
from jax import lax
from jax.sharding import PartitionSpec as P


def right_product(left, right):
    return lax.dot_general(
        left, right, (((1,), (1,)), ((), ())), preferred_element_type=jnp.float32
    )


def left_product(left, right):
    return lax.dot_general(
        left, right, (((0,), (0,)), ((), ())), preferred_element_type=jnp.float32
    )


def per_device(normed_input, cotangent, up_weight, down_weight):
    whole_input, whole_cot = (
        lax.all_gather(normed_input, "tp", axis=1, tiled=True),
        lax.all_gather(cotangent, "tp", axis=1, tiled=True),
    )
    rows = whole_input.shape[0]
    tokens = rows * lax.axis_size("fs")
    scale = lax.rsqrt(jnp.asarray(tokens, jnp.float32))
    block = whole_cot
    act_grad = right_product(block, lax.all_gather(down_weight, "fs", axis=1, tiled=True))
    whole_up = lax.all_gather(up_weight, "fs", axis=0, tiled=True)
    pre = jnp.dot(whole_input, whole_up, preferred_element_type=jnp.float32)
    rectified = jax.nn.relu(pre)
    act = (rectified * rectified).astype(jnp.bfloat16)
    pre_grad = (2.0 * rectified * act_grad).astype(jnp.bfloat16)
    partial_value = right_product(pre_grad, whole_up)
    input_grad = lax.psum_scatter(
        partial_value.astype(jnp.bfloat16), "tp", scatter_dimension=1, tiled=True
    )
    block = whole_input
    up_grad = lax.psum_scatter(
        (left_product(block, pre_grad) * scale).astype(jnp.bfloat16),
        "fs",
        scatter_dimension=0,
        tiled=True,
    ).astype(jnp.float32)
    down_term = left_product(act, whole_cot) * scale
    down_grad = lax.psum_scatter(
        down_term.astype(jnp.bfloat16), "fs", scatter_dimension=1, tiled=True
    ).astype(jnp.float32)
    return (input_grad, up_grad, down_grad)


def solution(mesh):
    in_specs = (P("fs", "tp"), P("fs", "tp"), P("fs", "tp"), P("tp", "fs"))
    out_specs = (P("fs", "tp"), P("fs", "tp"), P("tp", "fs"))
    return jax.shard_map(
        per_device, mesh=mesh, in_specs=in_specs, out_specs=out_specs, check_vma=False
    )
```

profile of v0, /device:TPU:0, one launch (start us, length us, event | category | flops | bytes accessed | tf_op | source)
XLA Modules:
  0.0 1207.0 jit_solution(5225547359864163482)
XLA Ops:
  7.2 0.0 all-gather.5.cloned.1.call-start
  7.2 0.7 all-gather.5.cloned.1.call-update
  7.9 0.0 all-gather.7.cloned.1.call-start
  7.9 0.7 all-gather.7.cloned.1.call-update
  8.6 0.0 all-gather.9.cloned.1.call-start
  8.7 0.7 all-gather.9.cloned.1.call-update
  9.4 0.0 all-gather.11.cloned.1.call-start
  9.4 0.5 all-gather.11.cloned.1.call-update
  10.0 0.0 reduce-scatter.12.cloned.1.call-start
  10.0 12.8 %all-gather.5.cloned.1.call-done = bf16[512,2048]{1,0:T(8,128)(2,1)} async-done(((bf16[512,1024]{1,0:T(8,128)(2,1)}), bf16[512,2048]{1,0:T(8,128)(2,1)}) %all-gather.5.cloned.1.call-update) | async-done | bytes 2097168 | tf_op jit(solution)/shard_map/all_gather | solution.py:21
  22.8 195.0 %all-gather.7.cloned.1.call-done = bf16[2048,4096]{1,0:T(8,128)(2,1)} async-done(((bf16[128,4096]{1,0:T(8,128)(2,1)}), bf16[2048,4096]{1,0:T(8,128)(2,1)}) %all-gather.7.cloned.1.call-update) | async-done | bytes 16777232 | tf_op jit(solution)/shard_map/all_gather | solution.py:29
  217.8 14.9 %fusion.3 = f32[512,4096]{1,0:T(8,128)} fusion(bf16[512,2048]{1,0:T(8,128)(2,1)} %all-gather.5.cloned.1.call-done, bf16[2048,4096]{1,0:T(8,128)(2,1)} %all-gather.7.cloned.1.call-done), kind=kOutput, calls=%fused_computation.8 | convolution fusion | flops 8589934592 | bytes 27262976 | tf_op jit(solution)/shard_map/dot_general | solution.py:30
  232.7 16.2 %multiply_convert_fusion = bf16[4096,2048]{1,0:T(8,128)(2,1)} fusion(bf16[512,2048]{1,0:T(8,128)(2,1)} %all-gather.9.cloned.1.call-done, f32[512,4096]{1,0:T(8,128)} %fusion.3), kind=kOutput, calls=%fused_computation | convolution fusion | flops 8613003264 | bytes 27262976 | tf_op jit(solution)/shard_map/dot_general | solution.py:14
  248.9 21.5 %copy.11 = bf16[4096,2048]{0,1:T(8,128)(2,1)} copy(bf16[4096,2048]{1,0:T(8,128)(2,1)} %multiply_convert_fusion) | data formatting | bytes 33554432
  270.4 0.0 reduce-scatter.12.cloned.1.call-update
  270.5 0.0 copy-start
  270.5 0.2 reduce-scatter.10.cloned.1.call-start
  270.7 210.3 %all-gather.11.cloned.1.call-done = bf16[4096,2048]{1,0:T(8,128)(2,1)} async-done(((bf16[4096,128]{1,0:T(8,128)(2,1)}), bf16[4096,2048]{1,0:T(8,128)(2,1)}) %all-gather.11.cloned.1.call-update) | async-done | bytes 16777232 | tf_op jit(solution)/shard_map/all_gather | solution.py:28
  481.0 15.6 %multiply_convert_fusion.3 = bf16[512,4096]{1,0:T(8,128)(2,1)} fusion(f32[512,4096]{1,0:T(8,128)} %fusion.3, bf16[512,2048]{1,0:T(8,128)(2,1)} %all-gather.9.cloned.1.call-done, bf16[4096,2048]{1,0:T(8,128)(2,1)} %all-gather.11.cloned.1.call-done), kind=kOutput, calls=%fused_computation.4 | convolution fusion | flops 8598323200 | bytes 31457280 | tf_op jit(solution)/shard_map/dot_general | solution.py:8
  496.6 14.8 %fusion = bf16[2048,4096]{0,1:T(8,128)(2,1)} fusion(bf16[512,4096]{1,0:T(8,128)(2,1)} %multiply_convert_fusion.3, bf16[512,2048]{1,0:T(8,128)(2,1)S(1)} %copy-done), kind=kOutput, calls=%fused_computation.2 | convolution fusion | flops 8606711808 | bytes 23068672 | tf_op jit(solution)/shard_map/dot_general | solution.py:14
  511.4 21.4 %copy.9 = bf16[2048,4096]{1,0:T(8,128)(2,1)} copy(bf16[2048,4096]{0,1:T(8,128)(2,1)} %fusion) | data formatting | bytes 33554432
  532.8 0.0 reduce-scatter.10.cloned.1.call-update
  532.8 0.3 reduce-scatter.8.cloned.1.call-start
  533.1 14.8 %convolution_convert_fusion = bf16[512,2048]{1,0:T(8,128)(2,1)} fusion(bf16[512,4096]{1,0:T(8,128)(2,1)} %multiply_convert_fusion.3, bf16[2048,4096]{1,0:T(8,128)(2,1)} %all-gather.7.cloned.1.call-done), kind=kOutput, calls=%fused_computation.6 | convolution fusion | flops 8590983168 | bytes 23068672 | tf_op jit(solution)/shard_map/dot_general | solution.py:8
  547.9 0.0 reduce-scatter.8.cloned.1.call-update
  547.9 279.9 %reduce-scatter.12.cloned.1.call-done = bf16[128,4096]{1,0:T(8,128)(2,1)} async-done(((bf16[2048,4096]{1,0:T(8,128)(2,1)}), bf16[128,4096]{1,0:T(8,128)(2,1)}) %reduce-scatter.12.cloned.1.call-update) | async-done | bytes 1048592
  827.8 1.6 copy.12
  829.4 1.5 convert_element_type.31
  830.9 351.1 %reduce-scatter.10.cloned.1.call-done = bf16[128,4096]{1,0:T(8,128)(2,1)} async-done(((bf16[2048,4096]{1,0:T(8,128)(2,1)}), bf16[128,4096]{1,0:T(8,128)(2,1)}) %reduce-scatter.10.cloned.1.call-update) | async-done | bytes 1048592
  1182.0 1.6 copy.10
  1183.6 1.6 copy.8
  1185.3 14.9 %reduce-scatter.8.cloned.1.call-done = bf16[512,1024]{1,0:T(8,128)(2,1)} async-done(((bf16[512,2048]{1,0:T(8,128)(2,1)}), bf16[512,1024]{1,0:T(8,128)(2,1)}) %reduce-scatter.8.cloned.1.call-update) | async-done | bytes 1048592 | tf_op jit(solution)/shard_map/reduce_scatter | solution.py:35
  (2 shorter events, 0.0 us)
Async XLA Ops:
  7.2 15.7 %all-gather.5.cloned.1.call-start = ((), (), s32[]{:S(2)}) async-start(), calls=%async_computation.3 | async-start | bytes 3145728 | tf_op jit(solution)/shard_map/all_gather | solution.py:21
  7.9 209.9 %all-gather.7.cloned.1.call-start = ((), (), s32[]{:S(2)}) async-start(), calls=%async_computation.4 | async-start | bytes 17825792 | tf_op jit(solution)/shard_map/all_gather | solution.py:29
  8.6 224.1 %all-gather.9.cloned.1.call-start = ((), (), s32[]{:S(2)}) async-start(), calls=%async_computation.5 | async-start | bytes 3145728 | tf_op jit(solution)/shard_map/all_gather | solution.py:22
  9.4 471.7 %all-gather.11.cloned.1.call-start = ((), (), s32[]{:S(2)}) async-start(), calls=%async_computation.6 | async-start | bytes 17825792 | tf_op jit(solution)/shard_map/all_gather | solution.py:28
  10.0 817.9 %reduce-scatter.12.cloned.1.call-start = ((), (), s32[]{:S(2)}) async-start(), calls=%async_computation.9 | async-start | bytes 17825792
  270.5 226.2 %copy-start = (bf16[512,2048]{1,0:T(8,128)(2,1)S(1)}, bf16[512,2048]{1,0:T(8,128)(2,1)}, u32[]{:S(2)}) copy-start(bf16[512,2048]{1,0:T(8,128)(2,1)} %all-gather.5.cloned.1.call-done) | copy-start | bytes 6291460
  270.5 911.5 %reduce-scatter.10.cloned.1.call-start = ((), (), s32[]{:S(2)}) async-start(), calls=%async_computation.8 | async-start | bytes 17825792
  532.8 667.3 %reduce-scatter.8.cloned.1.call-start = ((), (), s32[]{:S(2)}) async-start(), calls=%async_computation.7 | async-start | bytes 3145728 | tf_op jit(solution)/shard_map/reduce_scatter | solution.py:35
Sparse Core Ops, SparseCore 0:
  9.5 13.2 all-gather.4
  25.6 192.1 all-gather.6
  219.4 8.7 all-gather.8
  230.7 250.2 all-gather.10
  483.2 344.5 reduce-scatter.11
  830.0 352.0 reduce-scatter.9
  1184.8 15.2 reduce-scatter.7
where the time goes:
time: 1210 us
  waiting for transfers between devices  1070 us (88%)
  matrix products  76.2 us (6%)
  local copies, waits for them, and re-layouts  47.8 us (4%)
  between operations  14.2 us (1%)
    unnamed x9, waiting for transfers between devices  634 us
    all_gather x1, waiting for transfers between devices, per_device(): lax.all_gather(down_weight, 'fs', axis=1, tiled=True)  210 us
    all_gather x1, waiting for transfers between devices, per_device(): whole_up = lax.all_gather(up_weight, 'fs', axis=0, tiled=True)  195 us
    unnamed x7, local copies, waits for them, and re-layouts  47.8 us
    dot_general x2, matrix products, left_product(): lax.dot_general(left, right, (((0,), (0,)), ((), ())), preferred_element_...  30.9 us
    dot_general x2, matrix products, right_product(): lax.dot_general(left, right, (((1,), (1,)), ((), ())), preferred_element_...  30.4 us
  transfers between devices with their start and end apart: 7, of which 6 were waited for; matrix products, arithmetic and copies ran while one was open for 10% of the time, Pallas kernels for 0%

commit v1 on v0

--- a/solution.py
+++ b/solution.py
@@ -26,7 +26,14 @@
     scale = lax.rsqrt(jnp.asarray(tokens, jnp.float32))
     block = whole_cot
     act_grad = right_product(block, lax.all_gather(down_weight, "fs", axis=1, tiled=True))
-    whole_up = lax.all_gather(up_weight, "fs", axis=0, tiled=True)
+    size = lax.axis_size("fs")
+    route = [(i, (i + 1) % size) for i in range(size)]
+    terms = [up_weight]
+    for far in range(1, size):
+        terms = [lax.ppermute(terms[0], "fs", route), *terms]
+    whole = jnp.concatenate(terms, axis=0)
+    places = (lax.axis_index("fs") + 1) * terms[-1].shape[0]
+    whole_up = jnp.roll(whole, places, axis=0)
     pre = jnp.dot(whole_input, whole_up, preferred_element_type=jnp.float32)
     rectified = jax.nn.relu(pre)
     act = (rectified * rectified).astype(jnp.bfloat16)

time: 1210 us -> 1310 us (1.083)
  local copies, waits for them, and re-layouts: 47.8 us -> 112 us
  waiting for transfers between devices: 1070 us -> 1090 us
  starting transfers between devices: 0.67 us -> 18.6 us
    ppermute x0 -> x15, waiting for transfers between devices: none -> 431 us  [per_device(): terms = [lax.ppermute(terms[0], 'fs', route), *terms]]
    all_gather x1, waiting for transfers between devices: 210 us -> 0.02 us  [per_device(): lax.all_gather(down_weight, 'fs', axis=1, tiled=True)]
    all_gather x1 -> x0, waiting for transfers between devices: 195 us -> none  [per_device(): whole_up = lax.all_gather(up_weight, 'fs', axis=0, tiled=True)]
    unnamed x7 -> x82, local copies, waits for them, and re-layouts: 47.8 us -> 111 us
    ppermute x0 -> x15, starting transfers between devices: none -> 18.4 us  [per_device(): terms = [lax.ppermute(terms[0], 'fs', route), *terms]]
    unnamed x9 -> x8, waiting for transfers between devices: 634 us -> 644 us
  transfers between devices with their start and end apart: 7 -> 21, of which waited for: 6 -> 18; matrix products, arithmetic and copies ran while one was open for 10% -> 14% of each run, Pallas kernels for 0% -> 0%
where the time goes in v1:
time: 1310 us
  waiting for transfers between devices  1090 us (83%)
  local copies, waits for them, and re-layouts  112 us (9%)
  matrix products  75.8 us (6%)
  starting transfers between devices  18.6 us (1%)
  between operations  14.3 us (1%)
    unnamed x8, waiting for transfers between devices  644 us
    ppermute x15, waiting for transfers between devices, per_device(): terms = [lax.ppermute(terms[0], 'fs', route), *terms]  431 us
    unnamed x82, local copies, waits for them, and re-layouts  111 us
    dot_general x2, matrix products, right_product(): lax.dot_general(left, right, (((1,), (1,)), ((), ())), preferred_element_...  32.6 us
    dot_general x2, matrix products, left_product(): lax.dot_general(left, right, (((0,), (0,)), ((), ())), preferred_element_...  27.9 us
  transfers between devices with their start and end apart: 21, of which 18 were waited for; matrix products, arithmetic and copies ran while one was open for 14% of the time, Pallas kernels for 0%

profile of v1, /device:TPU:0, one launch (start us, length us, event | category | flops | bytes accessed | tf_op | source)
XLA Modules:
  0.0 1312.1 jit_solution(5412112724794067305)
XLA Ops:
  8.0 3.0 collective-permute-start
  11.0 27.3 %collective-permute-done = bf16[128,4096]{1,0:T(8,128)(2,1)S(1)} collective-permute-done((bf16[128,4096]{1,0:T(8,128)(2,1)}, bf16[128,4096]{1,0:T(8,128)(2,1)S(1)}, u32[]{:S(2)}, u32[]{:S(2)}) %collective-permute-start) | collective-permute-done | bytes 1048608 | tf_op jit(solution)/shard_map/ppermute | solution.py:33
  38.3 27.9 %collective-permute-done.1 = bf16[128,4096]{1,0:T(8,128)(2,1)S(1)} collective-permute-done((bf16[128,4096]{1,0:T(8,128)(2,1)S(1)}, bf16[128,4096]{1,0:T(8,128)(2,1)S(1)}, u32[]{:S(2)}, u32[]{:S(2)}) %collective-permute-start.1) | collective-permute-done | bytes 1048608 | tf_op jit(solution)/shard_map/ppermute | solution.py:33
  66.3 33.7 %collective-permute-done.2 = bf16[128,4096]{1,0:T(8,128)(2,1)} collective-permute-done((bf16[128,4096]{1,0:T(8,128)(2,1)S(1)}, bf16[128,4096]{1,0:T(8,128)(2,1)}, u32[]{:S(2)}, u32[]{:S(2)}) %collective-permute-start.2) | collective-permute-done | bytes 1048608 | tf_op jit(solution)/shard_map/ppermute | solution.py:33
  100.0 2.6 collective-permute-start.3
  102.6 20.2 %collective-permute-done.3 = bf16[128,4096]{1,0:T(8,128)(2,1)S(1)} collective-permute-done((bf16[128,4096]{1,0:T(8,128)(2,1)}, bf16[128,4096]{1,0:T(8,128)(2,1)S(1)}, u32[]{:S(2)}, u32[]{:S(2)}) %collective-permute-start.3) | collective-permute-done | bytes 1048608 | tf_op jit(solution)/shard_map/ppermute | solution.py:33
  123.8 2.4 collective-permute-start.4
  126.2 20.1 %collective-permute-done.4 = bf16[128,4096]{1,0:T(8,128)(2,1)S(1)} collective-permute-done((bf16[128,4096]{1,0:T(8,128)(2,1)S(1)}, bf16[128,4096]{1,0:T(8,128)(2,1)S(1)}, u32[]{:S(2)}, u32[]{:S(2)}) %collective-permute-start.4) | collective-permute-done | bytes 1048608 | tf_op jit(solution)/shard_map/ppermute | solution.py:33
  149.5 20.2 %collective-permute-done.5 = bf16[128,4096]{1,0:T(8,128)(2,1)S(1)} collective-permute-done((bf16[128,4096]{1,0:T(8,128)(2,1)S(1)}, bf16[128,4096]{1,0:T(8,128)(2,1)S(1)}, u32[]{:S(2)}, u32[]{:S(2)}) %collective-permute-start.5) | collective-permute-done | bytes 1048608 | tf_op jit(solution)/shard_map/ppermute | solution.py:33
  172.8 20.3 %collective-permute-done.6 = bf16[128,4096]{1,0:T(8,128)(2,1)S(1)} collective-permute-done((bf16[128,4096]{1,0:T(8,128)(2,1)S(1)}, bf16[128,4096]{1,0:T(8,128)(2,1)S(1)}, u32[]{:S(2)}, u32[]{:S(2)}) %collective-permute-start.6) | collective-permute-done | bytes 1048608 | tf_op jit(solution)/shard_map/ppermute | solution.py:33
  196.1 20.3 %collective-permute-done.7 = bf16[128,4096]{1,0:T(8,128)(2,1)S(1)} collective-permute-done((bf16[128,4096]{1,0:T(8,128)(2,1)S(1)}, bf16[128,4096]{1,0:T(8,128)(2,1)S(1)}, u32[]{:S(2)}, u32[]{:S(2)}) %collective-permute-start.7) | collective-permute-done | bytes 1048608 | tf_op jit(solution)/shard_map/ppermute | solution.py:33
  219.5 20.7 %collective-permute-done.8 = bf16[128,4096]{1,0:T(8,128)(2,1)S(1)} collective-permute-done((bf16[128,4096]{1,0:T(8,128)(2,1)S(1)}, bf16[128,4096]{1,0:T(8,128)(2,1)S(1)}, u32[]{:S(2)}, u32[]{:S(2)}) %collective-permute-start.8) | collective-permute-done | bytes 1048608 | tf_op jit(solution)/shard_map/ppermute | solution.py:33
  242.8 22.1 %collective-permute-done.9 = bf16[128,4096]{1,0:T(8,128)(2,1)S(1)} collective-permute-done((bf16[128,4096]{1,0:T(8,128)(2,1)S(1)}, bf16[128,4096]{1,0:T(8,128)(2,1)S(1)}, u32[]{:S(2)}, u32[]{:S(2)}) %collective-permute-start.9) | collective-permute-done | bytes 1048608 | tf_op jit(solution)/shard_map/ppermute | solution.py:33
  266.1 31.1 %collective-permute-done.10 = bf16[128,4096]{1,0:T(8,128)(2,1)S(1)} collective-permute-done((bf16[128,4096]{1,0:T(8,128)(2,1)S(1)}, bf16[128,4096]{1,0:T(8,128)(2,1)S(1)}, u32[]{:S(2)}, u32[]{:S(2)}) %collective-permute-start.10) | collective-permute-done | bytes 1048608 | tf_op jit(solution)/shard_map/ppermute | solution.py:33
  298.2 49.7 %collective-permute-done.11 = bf16[128,4096]{1,0:T(8,128)(2,1)S(1)} collective-permute-done((bf16[128,4096]{1,0:T(8,128)(2,1)S(1)}, bf16[128,4096]{1,0:T(8,128)(2,1)S(1)}, u32[]{:S(2)}, u32[]{:S(2)}) %collective-permute-start.11) | collective-permute-done | bytes 1048608 | tf_op jit(solution)/shard_map/ppermute | solution.py:33
  348.8 49.7 %collective-permute-done.12 = bf16[128,4096]{1,0:T(8,128)(2,1)S(1)} collective-permute-done((bf16[128,4096]{1,0:T(8,128)(2,1)S(1)}, bf16[128,4096]{1,0:T(8,128)(2,1)S(1)}, u32[]{:S(2)}, u32[]{:S(2)}) %collective-permute-start.12) | collective-permute-done | bytes 1048608 | tf_op jit(solution)/shard_map/ppermute | solution.py:33
  399.5 23.1 %collective-permute-done.13 = bf16[128,4096]{1,0:T(8,128)(2,1)} collective-permute-done((bf16[128,4096]{1,0:T(8,128)(2,1)S(1)}, bf16[128,4096]{1,0:T(8,128)(2,1)}, u32[]{:S(2)}, u32[]{:S(2)}) %collective-permute-start.13) | collective-permute-done | bytes 1048608 | tf_op jit(solution)/shard_map/ppermute | solution.py:33
  422.7 44.7 %collective-permute-done.14 = bf16[128,4096]{1,0:T(8,128)(2,1)} collective-permute-done((bf16[128,4096]{1,0:T(8,128)(2,1)}, bf16[128,4096]{1,0:T(8,128)(2,1)}, u32[]{:S(2)}, u32[]{:S(2)}) %collective-permute-start.14) | collective-permute-done | bytes 1048608 | tf_op jit(solution)/shard_map/ppermute | solution.py:33
  467.4 2.3 constant_dynamic-update-slice_fusion.31
  476.7 2.3 constant_dynamic-update-slice_fusion.27
  483.6 2.4 constant_dynamic-update-slice_fusion.24
  492.8 2.3 constant_dynamic-update-slice_fusion.20
  521.4 15.4 %fusion.2 = f32[4096,512]{1,0:T(8,128)} fusion(bf16[512,2048]{1,0:T(8,128)(2,1)} %all-gather.4.cloned.1.call-done, bf16[4096,4096]{1,0:T(8,128)(2,1)} %constant_dynamic-update-slice_fusion, s32[]{:T(128)S(6)} %select_n.14), kind=kOutput, calls=%fused_computation.4 | convolution fusion | flops 8589934592 | bytes 27262980 | tf_op jit(solution)/shard_map/dot_general | solution.py:37
  536.7 16.2 %multiply_convert_fusion = bf16[4096,2048]{1,0:T(8,128)(2,1)} fusion(bf16[512,2048]{1,0:T(8,128)(2,1)} %all-gather.6.cloned.1.call-done, f32[4096,512]{1,0:T(8,128)} %fusion.2), kind=kOutput, calls=%fused_computation | convolution fusion | flops 8613003264 | bytes 27262976 | tf_op jit(solution)/shard_map/dot_general | solution.py:14
  552.9 20.7 %copy.14 = bf16[4096,2048]{0,1:T(8,128)(2,1)} copy(bf16[4096,2048]{1,0:T(8,128)(2,1)} %multiply_convert_fusion) | data formatting | bytes 33554432
  573.7 17.5 %fusion.5 = bf16[512,4096]{0,1:T(8,128)(2,1)S(1)} fusion(f32[4096,512]{1,0:T(8,128)} %fusion.2, bf16[512,2048]{1,0:T(8,128)(2,1)} %all-gather.6.cloned.1.call-done, bf16[4096,2048]{1,0:T(8,128)(2,1)} %all-gather.8.cloned.1.call-done), kind=kOutput, calls=%fused_computation.8 | convolution fusion | flops 8598323200 | bytes 31457280 | tf_op jit(solution)/shard_map/dot_general | solution.py:8
  593.4 11.7 fusion.4
  605.1 20.8 %copy.12 = bf16[2048,4096]{1,0:T(8,128)(2,1)} copy(bf16[2048,4096]{0,1:T(8,128)(2,1)} %fusion.4) | data formatting | bytes 33554432
  626.0 15.1 %fusion.7 = bf16[512,2048]{1,0:T(8,128)(2,1)} fusion(bf16[512,4096]{0,1:T(8,128)(2,1)} %copy-done.22, bf16[4096,4096]{1,0:T(8,128)(2,1)} %constant_dynamic-update-slice_fusion, s32[]{:T(128)S(6)} %select_n.14), kind=kOutput, calls=%fused_computation.11 | convolution fusion | flops 8590983168 | bytes 23068676 | tf_op jit(solution)/shard_map/dot_general | solution.py:8
  641.1 292.0 %reduce-scatter.12.cloned.1.call-done = bf16[128,4096]{1,0:T(8,128)(2,1)} async-done(((bf16[2048,4096]{1,0:T(8,128)(2,1)}), bf16[128,4096]{1,0:T(8,128)(2,1)}) %reduce-scatter.12.cloned.1.call-update) | async-done | bytes 1048592
  936.2 351.2 %reduce-scatter.10.cloned.1.call-done = bf16[128,4096]{1,0:T(8,128)(2,1)} async-done(((bf16[2048,4096]{1,0:T(8,128)(2,1)}), bf16[128,4096]{1,0:T(8,128)(2,1)}) %reduce-scatter.10.cloned.1.call-update) | async-done | bytes 1048592
  1290.6 14.7 %reduce-scatter.8.cloned.1.call-done = bf16[512,1024]{1,0:T(8,128)(2,1)} async-done(((bf16[512,2048]{1,0:T(8,128)(2,1)}), bf16[512,1024]{1,0:T(8,128)(2,1)}) %reduce-scatter.8.cloned.1.call-update) | async-done | bytes 1048592 | tf_op jit(solution)/shard_map/reduce_scatter | solution.py:42
  (105 shorter events, 74.3 us)
Async XLA Ops:
  7.2 492.4 %copy-start = (bf16[128,4096]{1,0:T(8,128)(2,1)S(1)}, bf16[128,4096]{1,0:T(8,128)(2,1)}, u32[]{:S(2)}) copy-start(bf16[128,4096]{1,0:T(8,128)(2,1)} %param.6) | copy-start | bytes 3145732
  7.2 514.2 %all-gather.4.cloned.1.call-start = ((), (), s32[]{:S(2)}) async-start(), calls=%async_computation.3 | async-start | bytes 3145728 | tf_op jit(solution)/shard_map/all_gather | solution.py:21
  7.9 528.8 %all-gather.6.cloned.1.call-start = ((), (), s32[]{:S(2)}) async-start(), calls=%async_computation.4 | async-start | bytes 3145728 | tf_op jit(solution)/shard_map/all_gather | solution.py:22
  8.0 30.4 %collective-permute-start = (bf16[128,4096]{1,0:T(8,128)(2,1)}, bf16[128,4096]{1,0:T(8,128)(2,1)S(1)}, u32[]{:S(2)}, u32[]{:S(2)}) collective-permute-start(bf16[128,4096]{1,0:T(8,128)(2,1)} %param.6), channel_id=1, source_target_pairs={{0,2},{2,4},{4,6},{6,8},{8,10},{10,12},{12,14},{14,16},{16,18},{18... | collective-permute-start | bytes 3145736 | tf_op jit(solution)/shard_map/ppermute | solution.py:33
  11.0 562.7 %all-gather.8.cloned.1.call-start = ((), (), s32[]{:S(2)}) async-start(), calls=%async_computation.5 | async-start | bytes 17825792 | tf_op jit(solution)/shard_map/all_gather | solution.py:28
  38.3 27.9 %collective-permute-start.1 = (bf16[128,4096]{1,0:T(8,128)(2,1)S(1)}, bf16[128,4096]{1,0:T(8,128)(2,1)S(1)}, u32[]{:S(2)}, u32[]{:S(2)}) collective-permute-start(bf16[128,4096]{1,0:T(8,128)(2,1)S(1)} %collective-permute-done), channel_id=1, source_target_pairs={{0,2},{2,4},{4,6},{6,8},{8,10},{10,12},{12,14},{14,16},{16,18},{18... | collective-permute-start | bytes 3145736 | tf_op jit(solution)/shard_map/ppermute | solution.py:33
  66.3 33.8 %collective-permute-start.2 = (bf16[128,4096]{1,0:T(8,128)(2,1)S(1)}, bf16[128,4096]{1,0:T(8,128)(2,1)}, u32[]{:S(2)}, u32[]{:S(2)}) collective-permute-start(bf16[128,4096]{1,0:T(8,128)(2,1)S(1)} %collective-permute-done.1), channel_id=1, source_target_pairs={{0,2},{2,4},{4,6},{6,8},{8,10},{10,12},{12,14},{14,16},{16,18},{18... | collective-permute-start | bytes 3145736 | tf_op jit(solution)/shard_map/ppermute | solution.py:33
  66.3 866.8 %reduce-scatter.12.cloned.1.call-start = ((), (), s32[]{:S(2)}) async-start(), calls=%async_computation.8 | async-start | bytes 17825792
  100.0 22.8 %collective-permute-start.3 = (bf16[128,4096]{1,0:T(8,128)(2,1)}, bf16[128,4096]{1,0:T(8,128)(2,1)S(1)}, u32[]{:S(2)}, u32[]{:S(2)}) collective-permute-start(bf16[128,4096]{1,0:T(8,128)(2,1)} %collective-permute-done.2), channel_id=1, source_target_pairs={{0,2},{2,4},{4,6},{6,8},{8,10},{10,12},{12,14},{14,16},{16,18},{18... | collective-permute-start | bytes 3145736 | tf_op jit(solution)/shard_map/ppermute | solution.py:33
  123.8 22.4 %collective-permute-start.4 = (bf16[128,4096]{1,0:T(8,128)(2,1)S(1)}, bf16[128,4096]{1,0:T(8,128)(2,1)S(1)}, u32[]{:S(2)}, u32[]{:S(2)}) collective-permute-start(bf16[128,4096]{1,0:T(8,128)(2,1)S(1)} %collective-permute-done.3), channel_id=1, source_target_pairs={{0,2},{2,4},{4,6},{6,8},{8,10},{10,12},{12,14},{14,16},{16,18},{18... | collective-permute-start | bytes 3145736 | tf_op jit(solution)/shard_map/ppermute | solution.py:33
  147.2 22.4 %collective-permute-start.5 = (bf16[128,4096]{1,0:T(8,128)(2,1)S(1)}, bf16[128,4096]{1,0:T(8,128)(2,1)S(1)}, u32[]{:S(2)}, u32[]{:S(2)}) collective-permute-start(bf16[128,4096]{1,0:T(8,128)(2,1)S(1)} %collective-permute-done.4), channel_id=1, source_target_pairs={{0,2},{2,4},{4,6},{6,8},{8,10},{10,12},{12,14},{14,16},{16,18},{18... | collective-permute-start | bytes 3145736 | tf_op jit(solution)/shard_map/ppermute | solution.py:33
  170.6 22.4 %collective-permute-start.6 = (bf16[128,4096]{1,0:T(8,128)(2,1)S(1)}, bf16[128,4096]{1,0:T(8,128)(2,1)S(1)}, u32[]{:S(2)}, u32[]{:S(2)}) collective-permute-start(bf16[128,4096]{1,0:T(8,128)(2,1)S(1)} %collective-permute-done.5), channel_id=1, source_target_pairs={{0,2},{2,4},{4,6},{6,8},{8,10},{10,12},{12,14},{14,16},{16,18},{18... | collective-permute-start | bytes 3145736 | tf_op jit(solution)/shard_map/ppermute | solution.py:33
  194.1 22.4 %collective-permute-start.7 = (bf16[128,4096]{1,0:T(8,128)(2,1)S(1)}, bf16[128,4096]{1,0:T(8,128)(2,1)S(1)}, u32[]{:S(2)}, u32[]{:S(2)}) collective-permute-start(bf16[128,4096]{1,0:T(8,128)(2,1)S(1)} %collective-permute-done.6), channel_id=1, source_target_pairs={{0,2},{2,4},{4,6},{6,8},{8,10},{10,12},{12,14},{14,16},{16,18},{18... | collective-permute-start | bytes 3145736 | tf_op jit(solution)/shard_map/ppermute | solution.py:33
  217.5 22.6 %collective-permute-start.8 = (bf16[128,4096]{1,0:T(8,128)(2,1)S(1)}, bf16[128,4096]{1,0:T(8,128)(2,1)S(1)}, u32[]{:S(2)}, u32[]{:S(2)}) collective-permute-start(bf16[128,4096]{1,0:T(8,128)(2,1)S(1)} %collective-permute-done.7), channel_id=1, source_target_pairs={{0,2},{2,4},{4,6},{6,8},{8,10},{10,12},{12,14},{14,16},{16,18},{18... | collective-permute-start | bytes 3145736 | tf_op jit(solution)/shard_map/ppermute | solution.py:33
  241.1 23.8 %collective-permute-start.9 = (bf16[128,4096]{1,0:T(8,128)(2,1)S(1)}, bf16[128,4096]{1,0:T(8,128)(2,1)S(1)}, u32[]{:S(2)}, u32[]{:S(2)}) collective-permute-start(bf16[128,4096]{1,0:T(8,128)(2,1)S(1)} %collective-permute-done.8), channel_id=1, source_target_pairs={{0,2},{2,4},{4,6},{6,8},{8,10},{10,12},{12,14},{14,16},{16,18},{18... | collective-permute-start | bytes 3145736 | tf_op jit(solution)/shard_map/ppermute | solution.py:33
  265.9 31.3 %collective-permute-start.10 = (bf16[128,4096]{1,0:T(8,128)(2,1)S(1)}, bf16[128,4096]{1,0:T(8,128)(2,1)S(1)}, u32[]{:S(2)}, u32[]{:S(2)}) collective-permute-start(bf16[128,4096]{1,0:T(8,128)(2,1)S(1)} %collective-permute-done.9), channel_id=1, source_target_pairs={{0,2},{2,4},{4,6},{6,8},{8,10},{10,12},{12,14},{14,16},{16,18},{18... | collective-permute-start | bytes 3145736 | tf_op jit(solution)/shard_map/ppermute | solution.py:33
  298.2 49.7 %collective-permute-start.11 = (bf16[128,4096]{1,0:T(8,128)(2,1)S(1)}, bf16[128,4096]{1,0:T(8,128)(2,1)S(1)}, u32[]{:S(2)}, u32[]{:S(2)}) collective-permute-start(bf16[128,4096]{1,0:T(8,128)(2,1)S(1)} %collective-permute-done.10), channel_id=1, source_target_pairs={{0,2},{2,4},{4,6},{6,8},{8,10},{10,12},{12,14},{14,16},{16,18},{18... | collective-permute-start | bytes 3145736 | tf_op jit(solution)/shard_map/ppermute | solution.py:33
  348.8 49.7 %collective-permute-start.12 = (bf16[128,4096]{1,0:T(8,128)(2,1)S(1)}, bf16[128,4096]{1,0:T(8,128)(2,1)S(1)}, u32[]{:S(2)}, u32[]{:S(2)}) collective-permute-start(bf16[128,4096]{1,0:T(8,128)(2,1)S(1)} %collective-permute-done.11), channel_id=1, source_target_pairs={{0,2},{2,4},{4,6},{6,8},{8,10},{10,12},{12,14},{14,16},{16,18},{18... | collective-permute-start | bytes 3145736 | tf_op jit(solution)/shard_map/ppermute | solution.py:33
  399.5 23.1 %collective-permute-start.13 = (bf16[128,4096]{1,0:T(8,128)(2,1)S(1)}, bf16[128,4096]{1,0:T(8,128)(2,1)}, u32[]{:S(2)}, u32[]{:S(2)}) collective-permute-start(bf16[128,4096]{1,0:T(8,128)(2,1)S(1)} %collective-permute-done.12), channel_id=1, source_target_pairs={{0,2},{2,4},{4,6},{6,8},{8,10},{10,12},{12,14},{14,16},{16,18},{18... | collective-permute-start | bytes 3145736 | tf_op jit(solution)/shard_map/ppermute | solution.py:33
  422.6 44.8 %collective-permute-start.14 = (bf16[128,4096]{1,0:T(8,128)(2,1)}, bf16[128,4096]{1,0:T(8,128)(2,1)}, u32[]{:S(2)}, u32[]{:S(2)}) collective-permute-start(bf16[128,4096]{1,0:T(8,128)(2,1)} %collective-permute-done.13), channel_id=1, source_target_pairs={{0,2},{2,4},{4,6},{6,8},{8,10},{10,12},{12,14},{14,16},{16,18},{18... | collective-permute-start | bytes 3145736 | tf_op jit(solution)/shard_map/ppermute | solution.py:33
  422.6 82.6 %copy-start.20 = (bf16[128,4096]{1,0:T(8,128)(2,1)S(1)}, bf16[128,4096]{1,0:T(8,128)(2,1)}, u32[]{:S(2)}) copy-start(bf16[128,4096]{1,0:T(8,128)(2,1)} %copy-done.19) | copy-start | bytes 3145732
  422.6 83.7 %copy-start.18 = (bf16[128,4096]{1,0:T(8,128)(2,1)S(1)}, bf16[128,4096]{1,0:T(8,128)(2,1)}, u32[]{:S(2)}) copy-start(bf16[128,4096]{1,0:T(8,128)(2,1)} %copy-done.17) | copy-start | bytes 3145732
  422.6 84.7 %copy-start.16 = (bf16[128,4096]{1,0:T(8,128)(2,1)S(1)}, bf16[128,4096]{1,0:T(8,128)(2,1)}, u32[]{:S(2)}) copy-start(bf16[128,4096]{1,0:T(8,128)(2,1)} %copy-done.15) | copy-start | bytes 3145732
  422.6 85.8 %copy-start.14 = (bf16[128,4096]{1,0:T(8,128)(2,1)S(1)}, bf16[128,4096]{1,0:T(8,128)(2,1)}, u32[]{:S(2)}) copy-start(bf16[128,4096]{1,0:T(8,128)(2,1)} %copy-done.13) | copy-start | bytes 3145732
  422.6 86.8 %copy-start.12 = (bf16[128,4096]{1,0:T(8,128)(2,1)S(1)}, bf16[128,4096]{1,0:T(8,128)(2,1)}, u32[]{:S(2)}) copy-start(bf16[128,4096]{1,0:T(8,128)(2,1)} %copy-done.11) | copy-start | bytes 3145732
  422.6 87.9 %copy-start.10 = (bf16[128,4096]{1,0:T(8,128)(2,1)S(1)}, bf16[128,4096]{1,0:T(8,128)(2,1)}, u32[]{:S(2)}) copy-start(bf16[128,4096]{1,0:T(8,128)(2,1)} %copy-done.9) | copy-start | bytes 3145732
  422.6 89.0 %copy-start.8 = (bf16[128,4096]{1,0:T(8,128)(2,1)S(1)}, bf16[128,4096]{1,0:T(8,128)(2,1)}, u32[]{:S(2)}) copy-start(bf16[128,4096]{1,0:T(8,128)(2,1)} %copy-done.7) | copy-start | bytes 3145732
  422.6 90.0 %copy-start.6 = (bf16[128,4096]{1,0:T(8,128)(2,1)S(1)}, bf16[128,4096]{1,0:T(8,128)(2,1)}, u32[]{:S(2)}) copy-start(bf16[128,4096]{1,0:T(8,128)(2,1)} %copy-done.5) | copy-start | bytes 3145732
  422.7 91.0 %copy-start.4 = (bf16[128,4096]{1,0:T(8,128)(2,1)S(1)}, bf16[128,4096]{1,0:T(8,128)(2,1)}, u32[]{:S(2)}) copy-start(bf16[128,4096]{1,0:T(8,128)(2,1)} %copy-done.3) | copy-start | bytes 3145732
  422.7 92.1 %copy-start.2 = (bf16[128,4096]{1,0:T(8,128)(2,1)S(1)}, bf16[128,4096]{1,0:T(8,128)(2,1)}, u32[]{:S(2)}) copy-start(bf16[128,4096]{1,0:T(8,128)(2,1)} %copy-done.1) | copy-start | bytes 3145732
  573.6 713.7 %reduce-scatter.10.cloned.1.call-start = ((), (), s32[]{:S(2)}) async-start(), calls=%async_computation.7 | async-start | bytes 17825792
  625.9 679.4 %reduce-scatter.8.cloned.1.call-start = ((), (), s32[]{:S(2)}) async-start(), calls=%async_computation.6 | async-start | bytes 3145728 | tf_op jit(solution)/shard_map/reduce_scatter | solution.py:42
  (12 other events, 31.8 us)
Sparse Core Ops, SparseCore 0:
  9.5 13.2 all-gather.3
  24.4 11.7 all-gather.5
  66.4 498.3 all-gather.7
  573.7 359.3 reduce-scatter.11
  935.3 352.0 reduce-scatter.9
  1290.0 15.2 reduce-scatter.7
